TPU v7x, 256 devices: a whole 4x4x8 slice. The times are simulated.
256 devices in a mesh: sp: 32 (over z, x), tp: 4 (over y), dp: 2 (over core).
Axes of the slice: x: 4, y: 4, z: 8, core: 2. Of those that a mesh axis runs over, the one named last changes fastest.
Arguments:
- latents: bfloat16 [2, 8192, 4096], P('dp', ('sp', 'tp')), may hold values from -8 to 8
- cond: bfloat16 [2, 4096], P('dp', 'sp'), may hold values from -6 to 6
- cond_ctx: bfloat16 [4096], P('sp'), may hold values from -6 to 6
- context: bfloat16 [2, 1024, 4096], P('dp', 'sp'), may hold values from -8 to 8
- w_shift: bfloat16 [4096, 4096], P('sp', 'tp'), may hold values from -0.09375 to 0.09375
- w_scale: bfloat16 [4096, 4096], P('sp', 'tp'), may hold values from -0.09375 to 0.09375
- w_gate: bfloat16 [4096, 4096], P('sp', 'tp'), may hold values from -0.1875 to 0.1875
- gain_pre: bfloat16 [4096], replicated, may hold values from 0.099609375 to 1.8984375
- gain_post: bfloat16 [4096], replicated, may hold values from 0.099609375 to 1.8984375
- w_query: bfloat16 [4096, 1024], P('dp', 'tp'), may hold values from -0.09375 to 0.09375
- w_key: bfloat16 [4096, 1024], P('dp', 'tp'), may hold values from -0.09375 to 0.09375
- w_value: bfloat16 [4096, 2048], P('dp', 'tp'), may hold values from -0.09375 to 0.09375
- w_outgate: bfloat16 [4096, 2048], P('dp', 'tp'), may hold values from -0.09375 to 0.09375
- w_down: bfloat16 [4096, 32], replicated, may hold values from -0.25 to 0.25
- decay_up: bfloat16 [2, 16, 1024], P(None, None, 'tp'), may hold values from -1.5 to 1.5
- decay_bias: float32 [2, 1024], P(None, 'tp'), may hold values from -0.5 to 11
- head_gain: bfloat16 [2048], P('tp'), may hold values from 0.099609375 to 1.8984375
- w_out: bfloat16 [2048, 4096], P('tp', 'dp'), may hold values from -0.125 to 0.125
Outputs:
- mixer_out: bfloat16 [2, 8192, 4096], P('dp', ('sp', 'tp'))
All inputs are finite; a program needn't handle non-finite values.
Results may differ from a plain program's by a relative error of at most 0.015.
Values may be sent and summed in bfloat16 or wider, within the bound.
A program may use at most 128 MiB of HBM per device.

v0:
```python
import jax
import jax.numpy as jnp
from jax import lax
from jax.sharding import Mesh
from jax.sharding import PartitionSpec as P

DK_HEAD = 256
DV_HEAD = 512
RANK = 16
BLOCK = 128
SP_TP = ("sp_0", "sp_1", "tp")
SP = ("sp_0", "sp_1")
EPS = 1e-06
TAU = 16.0


def over_axes(value, axes):
    for axis in axes:
        value = lax.psum(value, axis)
    return value


def rows_first(arrays, axis, dims):
    turned = [jnp.moveaxis(a, dim, 0) for a, dim in zip(arrays, dims)]
    widths = [t[0].size for t in turned]
    both = jnp.concatenate([t.reshape(-1, w) for t, w in zip(turned, widths)], axis=1)
    result = lax.all_gather(both, axis, axis=0, tiled=True)
    tiles = jnp.split(result, [sum(widths[:k]) for k in range(1, len(widths))], axis=1)
    return tuple(
        (
            jnp.moveaxis(b.reshape(-1, *t.shape[1:]), 0, dim)
            for b, t, dim in zip(tiles, turned, dims)
        )
    )


def in_one_piece(arrays, axis, dim, along):
    ends, at = ([], 0)
    for a in arrays[:-1]:
        at += a.shape[along]
        ends.append(at)
    both = jnp.concatenate(arrays, axis=along)
    return tuple(jnp.split(lax.all_gather(both, axis, axis=dim, tiled=True), ends, axis=along))


def nothing_yet(value, identity):
    return jax.tree.map(
        lambda a, e: jnp.broadcast_to(jnp.asarray(e, a.dtype), a.shape), value, identity
    )


def prefix_by_axis(value, axes, combine, identity, reverse):
    before = start = nothing_yet(value, identity)
    total = value
    for axis in reversed(axes):
        count, mine = (lax.axis_size(axis), lax.axis_index(axis))
        pieces = jax.tree.map(lambda part: lax.all_gather(part, axis), total)
        inside, total = (start, start)
        for k in reversed(range(count)) if reverse else range(count):
            passed = k > mine if reverse else k < mine
            total = combine(total, jax.tree.map(lambda part: part[k], pieces))
            inside = jax.tree.map(lambda new, old: jnp.where(passed, new, old), total, inside)
        before = combine(inside, before)
    return before


def in_blocks(value, dim, count):
    lengths = value.shape
    tiles = value.reshape(*lengths[:dim], count, lengths[dim] // count, *lengths[dim + 1 :])
    return jnp.moveaxis(tiles, dim, 0)


def sent_and_summed(value, axis, dim):
    tiles = in_blocks(value, dim, lax.axis_size(axis))
    arrived = lax.all_to_all(tiles, axis, split_axis=0, concat_axis=0, tiled=True)
    return arrived.astype(jnp.float32).sum(axis=0)


def matmul(left, right):
    return jnp.dot(left, right, preferred_element_type=jnp.float32)


def rms_scale(vectors, gain):
    return vectors * lax.rsqrt(jnp.mean(vectors * vectors, axis=-1, keepdims=True) + EPS) * gain


def log_decays(lowrank, decay_up, decay_bias):
    result = []
    for direction in range(2):
        preact = (
            matmul(lowrank[:, direction * RANK : (direction + 1) * RANK], decay_up[direction])
            + decay_bias[direction]
        )
        result.append(jax.nn.log_sigmoid(preact) / TAU)
    return result


def chain(earlier, later):
    return (earlier[0] + later[0], earlier[1] * jnp.exp(later[0])[:, :, None] + later[1])


def reverse_rows(array):
    return jnp.flip(array, axis=1)


def local_pass(queries, keys_in, values, decays):
    heads_here, length, key_width = queries.shape
    count = length // BLOCK
    middle = BLOCK // 2

    def blocks(array):
        return jnp.moveaxis(array.reshape(heads_here, count, BLOCK, array.shape[-1]), 1, 0)

    causal = jnp.tril(jnp.ones((BLOCK, BLOCK), bool))

    def advance(carried_state, inputs):
        query_block_tile, key_block_tile, value_block_tile, block_g = inputs
        running_decay_sum = jnp.cumsum(block_g, axis=1)
        center = running_decay_sum[:, middle : middle + 1]
        scores = jnp.einsum(
            "htk,hsk->hts",
            query_block_tile * jnp.exp(running_decay_sum - center),
            key_block_tile * jnp.exp(center - running_decay_sum),
        )
        scores = jnp.where(causal, scores, 0.0)
        final_state_value = running_decay_sum[:, -1:]
        output = jnp.einsum("hts,hsv->htv", scores, value_block_tile) + jnp.einsum(
            "nyf,nfe->nye", query_block_tile * jnp.exp(running_decay_sum), carried_state
        )
        carried_state = carried_state * jnp.exp(final_state_value[:, 0])[:, :, None] + jnp.einsum(
            "dzg,dzu->dgu",
            key_block_tile * jnp.exp(final_state_value - running_decay_sum),
            value_block_tile,
        )
        return (carried_state, output)

    initial = jnp.zeros((heads_here, key_width, values.shape[-1]), jnp.float32)
    carried_state, output = lax.scan(
        advance, initial, (blocks(queries), blocks(keys_in), blocks(values), blocks(decays))
    )
    output = jnp.moveaxis(output, 0, 1).reshape(heads_here, length, values.shape[-1])
    return (output, carried_state, jnp.sum(decays, axis=1))


def body(
    latents,
    cond,
    cond_ctx,
    context,
    w_shift,
    w_scale,
    w_gate,
    gain_pre,
    gain_post,
    w_query,
    w_key,
    w_value,
    w_outgate,
    w_down,
    decay_up,
    decay_bias,
    head_gain,
    w_out,
):
    width = gain_pre.shape[0]
    column_count = w_shift.shape[1]
    column_start = lax.axis_index("tp") * column_count
    activated = jax.nn.silu(cond.astype(jnp.float32)).astype(jnp.bfloat16)
    activated_ctx = jax.nn.silu(cond_ctx.astype(jnp.float32)).astype(jnp.bfloat16)[None, :]

    def placed(part):
        return lax.dynamic_update_slice_in_dim(
            jnp.zeros((part.shape[0], width), jnp.float32), part, column_start, 1
        )

    shift_vec, scale_vec, gate_vec, shift_ctx, scale_ctx = (
        over_axes(placed(matmul(activated, w_shift)), SP_TP),
        over_axes(placed(matmul(activated, w_scale)), SP_TP),
        over_axes(placed(matmul(activated, w_gate)), SP_TP),
        over_axes(placed(matmul(activated_ctx, w_shift)), SP_TP),
        over_axes(placed(matmul(activated_ctx, w_scale)), SP_TP),
    )
    w_query, w_key, w_value, w_outgate, w_out = rows_first(
        (w_query, w_key, w_value, w_outgate, w_out), "dp", (0, 0, 0, 0, 1)
    )

    def project(rows, mats):
        return tuple((matmul(rows, weight).astype(jnp.bfloat16) for weight in mats))

    gain_in = gain_pre.astype(jnp.float32)
    latent_rows = latents[0].astype(jnp.float32)
    modulated = (rms_scale(latent_rows, gain_in) * (1.0 + scale_vec[0]) + shift_vec[0]).astype(
        jnp.bfloat16
    )
    lowrank = matmul(modulated, w_down).astype(jnp.bfloat16)
    all_rows, all_lowrank = in_one_piece((modulated, lowrank), "tp", 0, 1)
    queries, latent_keys, values, out_gate = project(all_rows, (w_query, w_key, w_value, w_outgate))
    decay_fwd, decay_bwd = log_decays(all_lowrank, decay_up, decay_bias)
    ctx_float = context[0].astype(jnp.float32)
    modulated_ctx = (rms_scale(ctx_float, gain_in) * (1.0 + scale_ctx[0]) + shift_ctx[0]).astype(
        jnp.bfloat16
    )
    keys_part, values_part = project(modulated_ctx, (w_key, w_value))
    ctx_keys, ctx_values, ctx_lowrank = in_one_piece(
        (keys_part, values_part, matmul(modulated_ctx, w_down).astype(jnp.bfloat16)), SP, 0, 1
    )
    heads_here = queries.shape[1] // DK_HEAD

    def by_head(array, head_width):
        return jnp.moveaxis(
            array.astype(jnp.float32).reshape(array.shape[0], heads_here, head_width), 1, 0
        )

    ctx_fwd, ctx_bwd = log_decays(ctx_lowrank, decay_up, decay_bias)
    ctx_head_keys = by_head(ctx_keys, DK_HEAD)
    ctx_head_values = by_head(ctx_values, DV_HEAD)
    ctx_head_fwd = by_head(ctx_fwd, DK_HEAD)
    ctx_head_bwd = by_head(ctx_bwd, DK_HEAD)
    ctx_cumulative = jnp.cumsum(ctx_head_fwd, axis=1)
    start_fwd = jnp.einsum(
        "dzg,dzu->dgu",
        ctx_head_keys * jnp.exp(ctx_cumulative[:, -1:] - ctx_cumulative),
        ctx_head_values,
    )
    start_bwd = jnp.einsum(
        "dzg,dzu->dgu",
        ctx_head_keys * jnp.exp(jnp.cumsum(ctx_head_bwd, axis=1) - ctx_head_bwd),
        ctx_head_values,
    )
    head_query_rows = by_head(queries, DK_HEAD) * DK_HEAD ** (-0.5)
    head_k = by_head(latent_keys, DK_HEAD)
    head_v = by_head(values, DV_HEAD)
    forward_head_output = by_head(decay_fwd, DK_HEAD)
    backward_head_output = reverse_rows(by_head(decay_bwd, DK_HEAD))
    out_fwd, state_fwd, total_fwd = local_pass(head_query_rows, head_k, head_v, forward_head_output)
    empty_pair = (jnp.zeros_like(total_fwd), jnp.zeros_like(state_fwd))
    prior_total, prior_state = prefix_by_axis((total_fwd, state_fwd), SP, chain, empty_pair, False)
    forward_entry_state = start_fwd * jnp.exp(prior_total)[:, :, None] + prior_state
    out_fwd = out_fwd + jnp.einsum(
        "nyf,nfe->nye",
        head_query_rows * jnp.exp(jnp.cumsum(forward_head_output, axis=1)),
        forward_entry_state,
    )
    reversed_query_rows = reverse_rows(head_query_rows)
    out_bwd, state_bwd, total_bwd = local_pass(
        reversed_query_rows, reverse_rows(head_k), reverse_rows(head_v), backward_head_output
    )
    later_total, later_state = prefix_by_axis((total_bwd, state_bwd), SP, chain, empty_pair, True)
    backward_entry_state = start_bwd * jnp.exp(later_total)[:, :, None] + later_state
    out_bwd = out_bwd + jnp.einsum(
        "nyf,nfe->nye",
        reversed_query_rows * jnp.exp(jnp.cumsum(backward_head_output, axis=1)),
        backward_entry_state,
    )
    mixed_sum = out_fwd + reverse_rows(out_bwd)
    gains_head = by_head(head_gain[None, :], DV_HEAD)
    gated_rows = rms_scale(mixed_sum, gains_head) * jax.nn.silu(by_head(out_gate, DV_HEAD))
    heads_out = (
        jnp.moveaxis(gated_rows, 0, 1)
        .reshape(gated_rows.shape[1], heads_here * DV_HEAD)
        .astype(jnp.bfloat16)
    )
    rounded = lax.optimization_barrier(matmul(heads_out, w_out).astype(jnp.bfloat16))
    projected = sent_and_summed(rounded.astype(jnp.float32).astype(jnp.bfloat16), "tp", 0)
    result_rows = latent_rows + gate_vec[0] * rms_scale(projected, gain_post.astype(jnp.float32))
    return result_rows.astype(jnp.bfloat16)[None]


def solution(mesh):
    finer = Mesh(
        mesh.devices.reshape(8, 4, mesh.shape["tp"], mesh.shape["dp"]), ("sp_0", "sp_1", "tp", "dp")
    )
    in_specs = (
        P("dp", SP_TP, None),
        P("dp", SP),
        P(SP),
        P("dp", SP, None),
        P(SP, "tp"),
        P(SP, "tp"),
        P(SP, "tp"),
        P(),
        P(),
        P("dp", "tp"),
        P("dp", "tp"),
        P("dp", "tp"),
        P("dp", "tp"),
        P(),
        P(None, None, "tp"),
        P(None, "tp"),
        P("tp"),
        P("tp", "dp"),
    )
    out_specs = P("dp", SP_TP, None)
    return jax.shard_map(body, mesh=finer, in_specs=in_specs, out_specs=out_specs, check_vma=False)
```

profile of v0, /device:TPU:2, one launch (start us, length us, event | category | flops | bytes accessed | tf_op | source)
XLA Modules:
  0.0 587.9 jit_solution(8418258431428282053)
XLA Ops:
  6.6 0.9 copy-done
  7.5 0.8 convolution_dynamic-update-slice_fusion.2
  8.3 1.1 convolution_dynamic-update-slice_fusion.3
  9.5 0.8 convolution_dynamic-update-slice_fusion
  10.3 1.1 convolution_dynamic-update-slice_fusion.1
  11.5 1.1 convolution_dynamic-update-slice_fusion.4
  13.3 74.2 %all-reduce.7.cloned.1.call-done = (f32[1,4096]{1,0:T(1,128)}, f32[1,4096]{1,0:T(1,128)}, f32[1,4096]{1,0:T(1,128)}, f32[1,4096]{1,0:T(1,128)}, f32[1,4096]{1,0:T(1,128)}) async-done(((f32[1,4096]{1,0:T(1,128)}, f32[1,4096]{1,0:T(1,128)}, f32[1,4096]{1,0:T(1,128)}, f32[1,4096]{1,0:T(1,128)}, f32[1,4096]{1,0:T(1,128)}), (f32[1,4096]{1,0:T(1,128)}, f32[1,4096]{1,0:T(1,128)}, f32[1,4096]{1,0:T(1,128)}, ...) | async-done | bytes 81936 | tf_op jit(solution)/shard_map/psum | solution.py:19
  87.6 1.2 fusion.174
  88.8 46.9 %all-reduce.11.cloned.1.call-done = (f32[1,4096]{1,0:T(1,128)}, f32[1,4096]{1,0:T(1,128)}, f32[1,4096]{1,0:T(1,128)}, f32[1,4096]{1,0:T(1,128)}, f32[1,4096]{1,0:T(1,128)}) async-done(((f32[1,4096]{1,0:T(1,128)}, f32[1,4096]{1,0:T(1,128)}, f32[1,4096]{1,0:T(1,128)}, f32[1,4096]{1,0:T(1,128)}, f32[1,4096]{1,0:T(1,128)}), (f32[1,4096]{1,0:T(1,128)}, f32[1,4096]{1,0:T(1,128)}, f32[1,4096]{1,0:T(1,128)}, ...) | async-done | bytes 81936 | tf_op jit(solution)/shard_map/psum | solution.py:19
  135.9 49.7 %all-reduce.9.cloned.1.call-done = (f32[4096]{0:T(1024)}, f32[1,4096]{1,0:T(1,128)}, f32[4096]{0:T(1024)}, f32[1,4096]{1,0:T(1,128)}, f32[4096]{0:T(1024)}) async-done(((f32[4096]{0:T(1024)}, f32[1,4096]{1,0:T(1,128)}, f32[4096]{0:T(1024)}, f32[1,4096]{1,0:T(1,128)}, f32[4096]{0:T(1024)}), (f32[4096]{0:T(1024)}, f32[1,4096]{1,0:T(1,128)}, f32[4096]{0:T(1024)}, f32[1,4096]{1,0:T(1,128)}, ...) | async-done | bytes 81936 | tf_op jit(solution)/shard_map/psum | solution.py:19
  186.3 1.0 fusion.178
  187.6 0.9 pad_maximum_fusion
  188.6 2.4 copy.41
  191.0 2.3 copy.42
  193.3 2.4 copy.43
  195.7 2.9 copy.44
  198.7 2.5 constant_dynamic-update-slice_fusion.3
  201.1 2.4 constant_dynamic-update-slice_fusion.2
  203.5 1.5 constant_dynamic-update-slice_fusion.1
  205.0 1.5 constant_dynamic-update-slice_fusion
  206.5 0.8 copy-done.7
  207.3 1.5 bitcast_dynamic-update-slice_fusion
  210.1 13.2 %all-gather.14.cloned.1.call-done = bf16[256,4128]{1,0:T(8,128)(2,1)} async-done(((bf16[64,4128]{1,0:T(8,128)(2,1)}), bf16[256,4128]{1,0:T(8,128)(2,1)}) %all-gather.14.cloned.1.call-update) | async-done | bytes 2113552 | tf_op jit(solution)/shard_map/all_gather | solution.py:43
  223.3 1.2 fusion.324
  224.7 35.7 %all-gather.16.cloned.1.call-done = bf16[4096,2048]{0,1:T(8,128)(2,1)} async-done(((bf16[2048,2048]{0,1:T(8,128)(2,1)}), bf16[4096,2048]{0,1:T(8,128)(2,1)}) %all-gather.16.cloned.1.call-update) | async-done | bytes 16777232 | tf_op jit(solution)/shard_map/all_gather | solution.py:27
  260.4 3.0 fusion.153
  263.5 4.1 fusion.131
  268.0 3.0 broadcast_multiply_fusion.2
  271.8 0.9 broadcast.715.clone
  272.7 3.5 while.27
  273.2 0.9 fusion.486
  275.0 0.9 fusion.486
  276.2 0.8 copy-done.2
  277.1 1.2 fusion.430
  278.3 2.1 while.26
  280.5 0.8 copy-done.3
  281.4 1.1 fusion.209
  283.3 1.4 convolution_convert_fusion.2
  284.7 2.5 fusion.171
  287.2 3.5 fusion.168
  291.4 8.0 %all-gather.5 = f32[4,1,256]{2,1,0:T(1,128)S(1)} all-gather(f32[1,1,256]{2,1,0:T(1,128)S(1)} %bitcast.746), channel_id=4, replica_groups=mesh['sp_0'=8,'sp_1'=4,'tp'=4,'dp'=2] {'sp_1'}, dimensions={0}, use_global_device_ids=true | all-gather | bytes 5120 | tf_op jit(solution)/shard_map/all_gather | solution.py:57
  299.5 11.4 %all-gather.26.cloned.1.call-done = f32[4,256,512]{2,1,0:T(8,128)} async-done(((f32[1,256,512]{2,1,0:T(8,128)}), f32[4,256,512]{2,1,0:T(8,128)}) %all-gather.26.cloned.1.call-update) | async-done | bytes 2097168 | tf_op jit(solution)/shard_map/all_gather | solution.py:57
  310.9 2.5 bitcast_add_fusion.6
  313.5 8.5 %all-gather.4 = f32[4,1,256]{2,1,0:T(1,128)S(1)} all-gather(f32[1,1,256]{2,1,0:T(1,128)S(1)} %bitcast.748), channel_id=2, replica_groups=mesh['sp_0'=8,'sp_1'=4,'tp'=4,'dp'=2] {'sp_1'}, dimensions={0}, use_global_device_ids=true | all-gather | bytes 5120 | tf_op jit(solution)/shard_map/all_gather | solution.py:57
  322.0 24.1 %all-gather.24.cloned.1.call-done = f32[4,256,512]{2,1,0:T(8,128)} async-done(((f32[1,256,512]{2,1,0:T(8,128)}), f32[4,256,512]{2,1,0:T(8,128)}) %all-gather.24.cloned.1.call-update) | async-done | bytes 2097168 | tf_op jit(solution)/shard_map/all_gather | solution.py:57
  346.1 2.5 bitcast_add_fusion.14
  349.5 16.6 %all_gather.60 = f32[8,1,256]{2,1,0:T(1,128)S(1)} all-gather(f32[1,1,256]{2,1,0:T(1,128)S(1)} %get-tuple-element.224), channel_id=1, replica_groups=mesh['sp_0'=8,'sp_1'=4,'tp'=4,'dp'=2] {'sp_0'}, dimensions={0}, use_global_device_ids=true | all-gather | bytes 9216 | tf_op jit(solution)/shard_map/all_gather | solution.py:57
  367.2 14.4 %all_gather.54 = f32[8,1,256]{2,1,0:T(1,128)S(1)} all-gather(f32[1,1,256]{2,1,0:T(1,128)S(1)} %get-tuple-element.220), channel_id=1, replica_groups=mesh['sp_0'=8,'sp_1'=4,'tp'=4,'dp'=2] {'sp_0'}, dimensions={0}, use_global_device_ids=true | all-gather | bytes 9216 | tf_op jit(solution)/shard_map/all_gather | solution.py:57
  384.5 41.4 %all-gather.18.cloned.1.call-done = bf16[1024,800]{1,0:T(8,128)(2,1)} async-done(((bf16[32,800]{1,0:T(8,128)(2,1)}), bf16[1024,800]{1,0:T(8,128)(2,1)}) %all-gather.18.cloned.1.call-update) | async-done | bytes 1638416 | tf_op jit(solution)/shard_map/all_gather | solution.py:43
  425.9 1.8 fusion.189
  428.8 1.7 fusion.187
  431.2 1.3 copy.52
  432.6 1.3 bitcast_add_fusion.1
  433.9 1.0 copy-done.8
  435.0 1.1 bitcast_add_fusion
  436.0 45.0 %all-gather.22.cloned.1.call-done = f32[8,1,256,512]{3,2,1,0:T(8,128)} async-done(((f32[1,1,256,512]{3,2,1,0:T(8,128)}), f32[8,1,256,512]{3,2,1,0:T(8,128)}) %all-gather.22.cloned.1.call-update) | async-done | bytes 4194320 | tf_op jit(solution)/shard_map/all_gather | solution.py:57
  481.1 6.1 %fusion.125 = f32[256,512]{1,0:T(8,128)} fusion(f32[256,512]{1,0:T(8,128)} %bitcast.715, f32[1,256,1024]{1,2,0:T(8,128)} %bitcast_add_fusion, f32[1024,256]{1,0:T(8,128)S(1)} %copy-done.11, bf16[1024,800]{1,0:T(8,128)(2,1)} %all-gather.18.cloned.1.call-done, f32[8,1,256,512]{3,2,1,0:T(8,128)} %all-gather.22.cloned.1.call-done, ...), kind=kOutput, calls=%fused_computation.130 | convolution fusion | flops 341573632 | bytes 11548684 | tf_op jit(solution)/shard_map/nyf,nfe->nye/dot_general | solution.py:250
  487.2 3.4 reverse.21
  490.6 45.4 %all-gather.20.cloned.1.call-done = f32[8,1,256,512]{3,2,1,0:T(8,128)} async-done(((f32[1,1,256,512]{3,2,1,0:T(8,128)}), f32[8,1,256,512]{3,2,1,0:T(8,128)}) %all-gather.20.cloned.1.call-update) | async-done | bytes 4194320 | tf_op jit(solution)/shard_map/all_gather | solution.py:57
  536.0 4.9 multiply_reduce_fusion.1
  541.0 8.0 %convolution_convert_fusion = bf16[256,4096]{1,0:T(8,128)(2,1)} fusion(bf16[4096,2048]{0,1:T(8,128)(2,1)} %all-gather.16.cloned.1.call-done, bf16[256,4128]{1,0:T(8,128)(2,1)} %all-gather.14.cloned.1.call-done, f32[256,512]{1,0:T(8,128)S(1)} %get-tuple-element.263, f32[512]{0:T(512)S(1)} %copy-done.36, f32[256]{0:T(256)S(1)} %add_rsqrt_fusion), kind=kOutput, calls=%fused_computation.90 | convolution fusion | flops 2149842944 | bytes 13110272 | tf_op jit(solution)/shard_map/dot_general | solution.py:80
  548.9 4.4 all-to-all-start
  553.4 26.2 %all-to-all-done = bf16[4,64,4096]{2,1,0:T(8,128)(2,1)S(1)} async-done(((bf16[4,64,4096]{2,1,0:T(8,128)(2,1)}), bf16[4,64,4096]{2,1,0:T(8,128)(2,1)S(1)}, u32[]{:S(2)}, u32[]{:S(2)}) %all-to-all-start) | async-done | bytes 2097184 | tf_op jit(solution)/shard_map/all_to_all | solution.py:75
  580.0 1.1 fusion.179
  (200 shorter events, 17.3 us)
Async XLA Ops:
  6.5 1.0 copy-start
  6.5 179.7 %copy-start.5 = (bf16[1,64,4096]{2,1,0:T(8,128)(2,1)S(1)}, bf16[1,64,4096]{2,1,0:T(8,128)(2,1)}, u32[]{:S(2)}) copy-start(bf16[1,64,4096]{2,1,0:T(8,128)(2,1)} %param.22) | copy-start | bytes 1572868
  6.5 129.3 %copy-start.26 = (bf16[4096]{0:T(1024)(128)(2,1)S(1)}, bf16[4096]{0:T(1024)(128)(2,1)}, u32[]{:S(2)}) copy-start(bf16[4096]{0:T(1024)(128)(2,1)} %param.29) | copy-start | bytes 24580
  6.5 180.7 %copy-start.13 = (bf16[4096,32]{0,1:T(8,128)(2,1)S(1)}, bf16[4096,32]{0,1:T(8,128)(2,1)}, u32[]{:S(2)}) copy-start(bf16[4096,32]{0,1:T(8,128)(2,1)} %param.35) | copy-start | bytes 786436
  6.5 80.9 %all-reduce.7.cloned.1.call-start = ((), (), s32[]{:S(2)}) async-start(), calls=%async_computation.8 | async-start | bytes 163840 | tf_op jit(solution)/shard_map/psum | solution.py:19
  8.3 4.3 copy-start.21
  9.5 3.1 copy-start.22
  10.3 2.3 copy-start.23
  11.5 1.2 copy-start.24
  12.6 0.6 copy-start.20
  13.2 122.5 %all-reduce.11.cloned.1.call-start = ((), (), s32[]{:S(2)}) async-start(), calls=%async_computation.10 | async-start | bytes 163840 | tf_op jit(solution)/shard_map/psum | solution.py:19
  87.5 98.0 %all-reduce.9.cloned.1.call-start = ((), (), s32[]{:S(2)}) async-start(), calls=%async_computation.9 | async-start | bytes 163840 | tf_op jit(solution)/shard_map/psum | solution.py:19
  135.8 87.5 %all-gather.14.cloned.1.call-start = ((), (), s32[]{:S(2)}) async-start(), calls=%async_computation.1 | async-start | bytes 2703360 | tf_op jit(solution)/shard_map/all_gather | solution.py:43
  135.9 55.1 %copy-start.18 = (f32[4096]{0:T(1024)}, f32[4096]{0:T(1024)S(1)}, u32[]{:S(2)}) copy-start(f32[4096]{0:T(1024)S(1)} %convert_element_type.101) | copy-start | bytes 49156
  188.5 4.8 copy-start.6
  188.5 71.9 %all-gather.16.cloned.1.call-start = ((), (), s32[]{:S(2)}) async-start(), calls=%async_computation.2 | async-start | bytes 25165824 | tf_op jit(solution)/shard_map/all_gather | solution.py:27
  198.7 4.9 copy-start.4
  205.0 2.3 copy-start.7
  208.9 0.7 copy-start.37
  208.9 14.4 %copy-start.46 = (bf16[2,16,256]{2,1,0:T(8,128)(2,1)S(1)}, bf16[2,16,256]{2,1,0:T(8,128)(2,1)}, u32[]{:S(2)}) copy-start(bf16[2,16,256]{2,1,0:T(8,128)(2,1)} %param.36) | copy-start | bytes 49156
  208.9 101.9 %all-gather.26.cloned.1.call-start = ((), (), s32[]{:S(2)}) async-start(), calls=%async_computation.7 | async-start | bytes 2621440 | tf_op jit(solution)/shard_map/all_gather | solution.py:57
  210.1 13.2 %copy-start.44 = (f32[1,256]{1,0:T(1,128)}, f32[1,256]{1,0:T(1,128)S(1)}, u32[]{:S(2)}) copy-start(f32[1,256]{1,0:T(1,128)S(1)} %get-tuple-element.257) | copy-start | bytes 3076
  271.0 0.7 copy-start.15
  276.2 0.8 copy-start.2
  277.0 69.0 %all-gather.24.cloned.1.call-start = ((), (), s32[]{:S(2)}) async-start(), calls=%async_computation.6 | async-start | bytes 2621440 | tf_op jit(solution)/shard_map/all_gather | solution.py:57
  280.5 0.8 copy-start.3
  280.5 6.6 %copy-start.12 = (f32[2,1,128,512]{3,2,1,0:T(8,128)}, f32[2,1,128,512]{3,2,1,0:T(8,128)S(1)}, u32[]{:S(2)}) copy-start(f32[2,1,128,512]{3,2,1,0:T(8,128)S(1)} %get-tuple-element.91) | copy-start | bytes 1572868
  281.3 5.8 copy-start.14
  281.3 5.8 copy-start.19
  281.3 5.8 copy-start.49
  281.3 144.6 %all-gather.18.cloned.1.call-start = ((), (), s32[]{:S(2)}) async-start(), calls=%async_computation.3 | async-start | bytes 1892352 | tf_op jit(solution)/shard_map/all_gather | solution.py:43
  291.4 189.6 %all-gather.22.cloned.1.call-start = ((), (), s32[]{:S(2)}) async-start(), calls=%async_computation.5 | async-start | bytes 4718592 | tf_op jit(solution)/shard_map/all_gather | solution.py:57
  299.4 14.0 %copy-start.28 = (f32[1,1,256]{2,1,0:T(1,128)}, f32[1,1,256]{2,1,0:T(1,128)S(1)}, u32[]{:S(2)}) copy-start(f32[1,1,256]{2,1,0:T(1,128)S(1)} %get-tuple-element.252) | copy-start | bytes 3076
  299.4 49.2 %copy-start.30 = (f32[1,1,256]{2,1,0:T(1,128)}, f32[1,1,256]{2,1,0:T(1,128)S(1)}, u32[]{:S(2)}) copy-start(f32[1,1,256]{2,1,0:T(1,128)S(1)} %get-tuple-element.253) | copy-start | bytes 3076
  299.4 49.1 %copy-start.32 = (f32[1,1,256]{2,1,0:T(1,128)}, f32[1,1,256]{2,1,0:T(1,128)S(1)}, u32[]{:S(2)}) copy-start(f32[1,1,256]{2,1,0:T(1,128)S(1)} %get-tuple-element.254) | copy-start | bytes 3076
  299.4 49.1 %copy-start.34 = (f32[1,1,256]{2,1,0:T(1,128)}, f32[1,1,256]{2,1,0:T(1,128)S(1)}, u32[]{:S(2)}) copy-start(f32[1,1,256]{2,1,0:T(1,128)S(1)} %get-tuple-element.255) | copy-start | bytes 3076
  313.4 35.3 %copy-start.38 = (bf16[512]{0:T(512)(128)(2,1)S(1)}, bf16[512]{0:T(512)(128)(2,1)}, u32[]{:S(2)}) copy-start(bf16[512]{0:T(512)(128)(2,1)} %param.38) | copy-start | bytes 3076
  313.4 222.6 %all-gather.20.cloned.1.call-start = ((), (), s32[]{:S(2)}) async-start(), calls=%async_computation.4 | async-start | bytes 4718592 | tf_op jit(solution)/shard_map/all_gather | solution.py:57
  348.6 77.3 %copy-start.45 = (f32[1,256]{1,0:T(1,128)S(1)}, f32[1,256]{1,0:T(1,128)}, u32[]{:S(2)}) copy-start(f32[1,256]{1,0:T(1,128)} %copy-done.44) | copy-start | bytes 3076
  348.6 77.3 %copy-start.47 = (bf16[2,16,256]{2,1,0:T(8,128)(2,1)S(1)}, bf16[2,16,256]{2,1,0:T(8,128)(2,1)}, u32[]{:S(2)}) copy-start(bf16[2,16,256]{2,1,0:T(8,128)(2,1)} %param.36) | copy-start | bytes 49156
  427.7 2.8 copy-start.10
  427.8 1.0 copy-start.43
  427.8 1.0 copy-start.48
  432.6 48.4 %copy-start.29 = (f32[1,1,256]{2,1,0:T(1,128)S(1)}, f32[1,1,256]{2,1,0:T(1,128)}, u32[]{:S(2)}) copy-start(f32[1,1,256]{2,1,0:T(1,128)} %copy-done.28) | copy-start | bytes 3076
  432.6 48.4 %copy-start.31 = (f32[1,1,256]{2,1,0:T(1,128)S(1)}, f32[1,1,256]{2,1,0:T(1,128)}, u32[]{:S(2)}) copy-start(f32[1,1,256]{2,1,0:T(1,128)} %copy-done.30) | copy-start | bytes 3076
  432.6 48.4 %copy-start.33 = (f32[1,1,256]{2,1,0:T(1,128)S(1)}, f32[1,1,256]{2,1,0:T(1,128)}, u32[]{:S(2)}) copy-start(f32[1,1,256]{2,1,0:T(1,128)} %copy-done.32) | copy-start | bytes 3076
  432.6 48.4 %copy-start.35 = (f32[1,1,256]{2,1,0:T(1,128)S(1)}, f32[1,1,256]{2,1,0:T(1,128)}, u32[]{:S(2)}) copy-start(f32[1,1,256]{2,1,0:T(1,128)} %copy-done.34) | copy-start | bytes 3076
  432.6 48.4 %copy-start.40 = (f32[1,1,256]{2,1,0:T(1,128)S(1)}, f32[1,1,256]{2,1,0:T(1,128)}, u32[]{:S(2)}) copy-start(f32[1,1,256]{2,1,0:T(1,128)} %get-tuple-element.222) | copy-start | bytes 3076
  432.6 48.4 %copy-start.42 = (f32[1,1,256]{2,1,0:T(1,128)S(1)}, f32[1,1,256]{2,1,0:T(1,128)}, u32[]{:S(2)}) copy-start(f32[1,1,256]{2,1,0:T(1,128)} %exp.529) | copy-start | bytes 3076
  433.9 1.0 copy-start.8
  434.9 46.1 %copy-start.11 = (f32[1024,256]{1,0:T(8,128)S(1)}, f32[1024,256]{1,0:T(8,128)}, u32[]{:S(2)}) copy-start(f32[1024,256]{1,0:T(8,128)} %copy-done.10) | copy-start | bytes 3145732
  481.0 55.0 %copy-start.9 = (f32[1,256,1024]{1,2,0:T(8,128)S(1)}, f32[1,256,1024]{1,2,0:T(8,128)}, u32[]{:S(2)}) copy-start(f32[1,256,1024]{1,2,0:T(8,128)} %copy-done.8) | copy-start | bytes 3145732
  481.0 55.0 %copy-start.16 = (f32[256,256]{1,0:T(8,128)S(1)}, f32[256,256]{1,0:T(8,128)}, u32[]{:S(2)}) copy-start(f32[256,256]{1,0:T(8,128)} %copy-done.15) | copy-start | bytes 786436
  481.1 55.0 %copy-start.17 = (f32[1,256,256]{1,2,0:T(8,128)S(1)}, f32[1,256,256]{1,2,0:T(8,128)}, u32[]{:S(2)}) copy-start(f32[1,256,256]{1,2,0:T(8,128)} %fusion.331) | copy-start | bytes 786436
  481.1 55.0 %copy-start.39 = (f32[1,1,256]{2,1,0:T(1,128)S(1)}, f32[1,1,256]{2,1,0:T(1,128)}, u32[]{:S(2)}) copy-start(f32[1,1,256]{2,1,0:T(1,128)} %get-tuple-element.218) | copy-start | bytes 3076
  481.1 55.0 %copy-start.41 = (f32[1,1,256]{2,1,0:T(1,128)S(1)}, f32[1,1,256]{2,1,0:T(1,128)}, u32[]{:S(2)}) copy-start(f32[1,1,256]{2,1,0:T(1,128)} %exp.528) | copy-start | bytes 3076
  536.0 4.9 copy-start.36
  548.9 4.4 copy-start.27
  548.9 30.6 %all-to-all-start = ((bf16[4,64,4096]{2,1,0:T(8,128)(2,1)}), bf16[4,64,4096]{2,1,0:T(8,128)(2,1)S(1)}, u32[]{:S(2)}, u32[]{:S(2)}) async-start(bf16[4,64,4096]{2,1,0:T(8,128)(2,1)} %bitcast.711), calls=%async_computation | async-start | bytes 4194304 | tf_op jit(solution)/shard_map/all_to_all | solution.py:75
  553.3 26.7 %copy-start.25 = (f32[4096]{0:T(1024)S(1)}, f32[4096]{0:T(1024)}, u32[]{:S(2)}) copy-start(f32[4096]{0:T(1024)} %get-tuple-element.212) | copy-start | bytes 49156
  579.5 1.6 copy-start.1
Sparse Core Ops, SparseCore 0:
  13.4 74.0 all-reduce.6
  90.2 45.5 all-reduce.10
  138.4 47.0 all-reduce.8
  188.6 34.5 all-gather.13
  224.9 35.4 all-gather.15
  277.1 33.6 all-gather.25
  312.7 33.3 all-gather.23
  348.6 77.2 all-gather.17
  427.7 53.2 all-gather.21
  482.6 53.3 all-gather.19
where the time goes:
time: 589 us; the launch traced here: 588 us
  waiting for transfers between devices  413 us (70%)
  matrix products  52.2 us (9%)
  blocking collectives  47.5 us (8%)
  local copies, waits for them, and re-layouts  34.5 us (6%)
  other arithmetic  21.2 us (4%)
  between operations  14.4 us (2%)
    psum x3, waiting for transfers between devices, over_axes(): value = lax.psum(value, axis)  171 us
    all_gather x4, waiting for transfers between devices, prefix_by_axis(): pieces = jax.tree.map(lambda part: lax.all_gather(part, axis), total)  126 us
    all_gather x2, waiting for transfers between devices, in_one_piece(): lax.all_gather(both, axis, axis=dim, tiled=True)  54.5 us
    all_gather x4, blocking collectives, prefix_by_axis(): pieces = jax.tree.map(lambda part: lax.all_gather(part, axis), total)  47.5 us
    dot_general x17, matrix products, matmul(): return jnp.dot(left, right, preferred_element_type=jnp.float32)  36.6 us
    all_gather x1, waiting for transfers between devices, rows_first(): result = lax.all_gather(both, axis, axis=0, tiled=True)  35.7 us
    all_to_all x1, waiting for transfers between devices, sent_and_summed(): lax.all_to_all(tiles, axis, split_axis=0, concat_axis=0, tiled=True)  26.2 us
    unnamed x108, local copies, waits for them, and re-layouts  24.2 us
  transfers between devices with their start and end apart: 11, of which 11 were waited for; matrix products, arithmetic and copies ran while one was open for 11% of the time, Pallas kernels for 0%

commit v1 on v0

--- a/solution.py
+++ b/solution.py
@@ -24,7 +24,9 @@
     turned = [jnp.moveaxis(a, dim, 0) for a, dim in zip(arrays, dims)]
     widths = [t[0].size for t in turned]
     both = jnp.concatenate([t.reshape(-1, w) for t, w in zip(turned, widths)], axis=1)
-    result = lax.all_gather(both, axis, axis=0, tiled=True)
+    result = jnp.concatenate(
+        lax.all_to_all(jnp.stack([both] * lax.axis_size(axis)), axis, 0, 0), axis=0
+    )
     tiles = jnp.split(result, [sum(widths[:k]) for k in range(1, len(widths))], axis=1)
     return tuple(
         (

time: 589 us -> 554 us (0.941)
  waiting for transfers between devices: 413 us -> 380 us
  local copies, waits for them, and re-layouts: 34.5 us -> 20.4 us
  starting transfers between devices: 4.82 us -> 14.6 us
    all_gather x1 -> x0, waiting for transfers between devices: 35.7 us -> none  [rows_first(): result = lax.all_gather(both, axis, axis=0, tiled=True)]
    unnamed x108 -> x75, local copies, waits for them, and re-layouts: 24.2 us -> 12.4 us
    all_to_all x0 -> x1, starting transfers between devices: none -> 9.86 us  [rows_first(): lax.all_to_all(jnp.stack([both] * lax.axis_size(axis)), axis, 0, 0)]
    another operation x10 -> x11, other arithmetic: 4.25 us -> 11 us  [the longest x1 6.76 us: rows_first(): jnp.stack([both] * lax.axis_size(axis))]
  transfers between devices with their start and end apart: 11 -> 11, of which waited for: 11 -> 11; matrix products, arithmetic and copies ran while one was open for 11% -> 10% of each run, Pallas kernels for 0% -> 0%
where the time goes in v1:
time: 554 us; the launch traced here: 553 us
  waiting for transfers between devices  380 us (69%)
  matrix products  51.1 us (9%)
  blocking collectives  47.5 us (9%)
  other arithmetic  25.7 us (5%)
  local copies, waits for them, and re-layouts  20.4 us (4%)
  starting transfers between devices  14.6 us (3%)
  between operations  14 us (3%)
    psum x3, waiting for transfers between devices, over_axes(): value = lax.psum(value, axis)  171 us
    all_gather x4, waiting for transfers between devices, prefix_by_axis(): pieces = jax.tree.map(lambda part: lax.all_gather(part, axis), total)  126 us
    all_gather x2, waiting for transfers between devices, in_one_piece(): lax.all_gather(both, axis, axis=dim, tiled=True)  54.1 us
    all_gather x4, blocking collectives, prefix_by_axis(): pieces = jax.tree.map(lambda part: lax.all_gather(part, axis), total)  47.5 us
    dot_general x17, matrix products, matmul(): return jnp.dot(left, right, preferred_element_type=jnp.float32)  35.7 us
    all_to_all x1, waiting for transfers between devices, sent_and_summed(): lax.all_to_all(tiles, axis, split_axis=0, concat_axis=0, tiled=True)  26.2 us
    unnamed x75, local copies, waits for them, and re-layouts  12.4 us
  transfers between devices with their start and end apart: 11, of which 11 were waited for; matrix products, arithmetic and copies ran while one was open for 10% of the time, Pallas kernels for 0%

profile of v1, /device:TPU:2, one launch (start us, length us, event | category | flops | bytes accessed | tf_op | source)
XLA Modules:
  0.0 553.1 jit_solution(17573487321284094099)
XLA Ops:
  6.6 0.9 copy-done
  7.5 0.8 convolution_dynamic-update-slice_fusion.2
  8.3 1.1 convolution_dynamic-update-slice_fusion.3
  9.5 0.8 convolution_dynamic-update-slice_fusion
  10.3 1.1 convolution_dynamic-update-slice_fusion.1
  11.5 1.1 convolution_dynamic-update-slice_fusion.4
  13.3 74.2 %all-reduce.7.cloned.1.call-done = (f32[1,4096]{1,0:T(1,128)}, f32[1,4096]{1,0:T(1,128)}, f32[1,4096]{1,0:T(1,128)}, f32[1,4096]{1,0:T(1,128)}, f32[1,4096]{1,0:T(1,128)}) async-done(((f32[1,4096]{1,0:T(1,128)}, f32[1,4096]{1,0:T(1,128)}, f32[1,4096]{1,0:T(1,128)}, f32[1,4096]{1,0:T(1,128)}, f32[1,4096]{1,0:T(1,128)}), (f32[1,4096]{1,0:T(1,128)}, f32[1,4096]{1,0:T(1,128)}, f32[1,4096]{1,0:T(1,128)}, ...) | async-done | bytes 81936 | tf_op jit(solution)/shard_map/psum | solution.py:19
  87.5 1.2 fusion.174
  88.8 46.9 %all-reduce.11.cloned.1.call-done = (f32[1,4096]{1,0:T(1,128)}, f32[1,4096]{1,0:T(1,128)}, f32[1,4096]{1,0:T(1,128)}, f32[1,4096]{1,0:T(1,128)}, f32[1,4096]{1,0:T(1,128)}) async-done(((f32[1,4096]{1,0:T(1,128)}, f32[1,4096]{1,0:T(1,128)}, f32[1,4096]{1,0:T(1,128)}, f32[1,4096]{1,0:T(1,128)}, f32[1,4096]{1,0:T(1,128)}), (f32[1,4096]{1,0:T(1,128)}, f32[1,4096]{1,0:T(1,128)}, f32[1,4096]{1,0:T(1,128)}, ...) | async-done | bytes 81936 | tf_op jit(solution)/shard_map/psum | solution.py:19
  135.9 49.7 %all-reduce.9.cloned.1.call-done = (f32[4096]{0:T(1024)}, f32[1,4096]{1,0:T(1,128)}, f32[4096]{0:T(1024)}, f32[1,4096]{1,0:T(1,128)}, f32[4096]{0:T(1024)}) async-done(((f32[4096]{0:T(1024)}, f32[1,4096]{1,0:T(1,128)}, f32[4096]{0:T(1024)}, f32[1,4096]{1,0:T(1,128)}, f32[4096]{0:T(1024)}), (f32[4096]{0:T(1024)}, f32[1,4096]{1,0:T(1,128)}, f32[4096]{0:T(1024)}, f32[1,4096]{1,0:T(1,128)}, ...) | async-done | bytes 81936 | tf_op jit(solution)/shard_map/psum | solution.py:19
  185.5 0.7 broadcast_add_fusion.1
  186.3 1.0 fusion.178
  187.6 0.9 pad_maximum_fusion.1
  188.5 2.9 copy.59
  191.4 1.5 constant_dynamic-update-slice_fusion.3
  192.9 1.4 constant_dynamic-update-slice_fusion.2
  194.6 1.3 copy-done.6
  196.6 6.8 %pad_maximum_fusion = bf16[2,2048,2048]{2,1,0:T(8,128)(2,1)} fusion(bf16[1,2048,2048]{2,1,0:T(8,128)(2,1)S(1)} %bitcast.703), kind=kLoop, calls=%fused_computation.90 | loop fusion | flops 8388608 | bytes 25165824 | tf_op jit(solution)/shard_map/stack | solution.py:28
  203.3 9.9 %all-to-all-start = ((bf16[2,2048,2048]{2,1,0:T(8,128)(2,1)}), bf16[2,2048,2048]{2,1,0:T(8,128)(2,1)}, u32[]{:S(2)}, u32[]{:S(2)}) async-start(bf16[2,2048,2048]{2,1,0:T(8,128)(2,1)} %pad_maximum_fusion), calls=%async_computation | async-start | bytes 33554432 | tf_op jit(solution)/shard_map/all_to_all | solution.py:28
  213.9 9.4 %all-gather.13.cloned.1.call-done = bf16[256,4128]{1,0:T(8,128)(2,1)} async-done(((bf16[64,4128]{1,0:T(8,128)(2,1)}), bf16[256,4128]{1,0:T(8,128)(2,1)}) %all-gather.13.cloned.1.call-update) | async-done | bytes 2113552 | tf_op jit(solution)/shard_map/all_gather | solution.py:45
  223.3 1.2 fusion.324
  224.7 2.0 all-to-all-done
  226.7 2.9 fusion.153
  229.8 4.1 fusion.131
  234.2 2.9 broadcast_multiply_fusion.2
  237.1 0.7 copy-done.14
  237.9 0.9 broadcast.715.clone
  238.8 3.5 while.27
  239.4 0.9 fusion.486
  241.1 0.9 fusion.486
  242.3 0.8 copy-done.2
  243.2 1.2 fusion.430
  244.5 2.1 while.26
  246.6 0.8 copy-done.3
  247.5 1.1 fusion.209
  248.7 0.7 broadcast_add_fusion
  249.4 1.4 convolution_convert_fusion.2
  250.8 2.2 fusion.171
  253.0 3.1 fusion.168
  256.8 8.0 %all-gather.5 = f32[4,1,256]{2,1,0:T(1,128)S(1)} all-gather(f32[1,1,256]{2,1,0:T(1,128)S(1)} %bitcast.749), channel_id=4, replica_groups=mesh['sp_0'=8,'sp_1'=4,'tp'=4,'dp'=2] {'sp_1'}, dimensions={0}, use_global_device_ids=true | all-gather | bytes 5120 | tf_op jit(solution)/shard_map/all_gather | solution.py:59
  264.8 11.7 %all-gather.23.cloned.1.call-done = f32[4,256,512]{2,1,0:T(8,128)} async-done(((f32[1,256,512]{2,1,0:T(8,128)}), f32[4,256,512]{2,1,0:T(8,128)}) %all-gather.23.cloned.1.call-update) | async-done | bytes 2097168 | tf_op jit(solution)/shard_map/all_gather | solution.py:59
  276.5 2.5 bitcast_add_fusion.6
  279.1 8.5 %all-gather.4 = f32[4,1,256]{2,1,0:T(1,128)S(1)} all-gather(f32[1,1,256]{2,1,0:T(1,128)S(1)} %bitcast.751), channel_id=2, replica_groups=mesh['sp_0'=8,'sp_1'=4,'tp'=4,'dp'=2] {'sp_1'}, dimensions={0}, use_global_device_ids=true | all-gather | bytes 5120 | tf_op jit(solution)/shard_map/all_gather | solution.py:59
  287.6 23.9 %all-gather.21.cloned.1.call-done = f32[4,256,512]{2,1,0:T(8,128)} async-done(((f32[1,256,512]{2,1,0:T(8,128)}), f32[4,256,512]{2,1,0:T(8,128)}) %all-gather.21.cloned.1.call-update) | async-done | bytes 2097168 | tf_op jit(solution)/shard_map/all_gather | solution.py:59
  311.5 2.5 bitcast_add_fusion.14
  314.4 16.6 %all_gather.56 = f32[8,1,256]{2,1,0:T(1,128)S(1)} all-gather(f32[1,1,256]{2,1,0:T(1,128)S(1)} %get-tuple-element.238), channel_id=1, replica_groups=mesh['sp_0'=8,'sp_1'=4,'tp'=4,'dp'=2] {'sp_0'}, dimensions={0}, use_global_device_ids=true | all-gather | bytes 9216 | tf_op jit(solution)/shard_map/all_gather | solution.py:59
  331.1 14.4 %all_gather.50 = f32[8,1,256]{2,1,0:T(1,128)S(1)} all-gather(f32[1,1,256]{2,1,0:T(1,128)S(1)} %get-tuple-element.234), channel_id=1, replica_groups=mesh['sp_0'=8,'sp_1'=4,'tp'=4,'dp'=2] {'sp_0'}, dimensions={0}, use_global_device_ids=true | all-gather | bytes 9216 | tf_op jit(solution)/shard_map/all_gather | solution.py:59
  345.8 0.7 fusion.328
  346.7 44.7 %all-gather.15.cloned.1.call-done = bf16[1024,800]{1,0:T(8,128)(2,1)} async-done(((bf16[32,800]{1,0:T(8,128)(2,1)}), bf16[1024,800]{1,0:T(8,128)(2,1)}) %all-gather.15.cloned.1.call-update) | async-done | bytes 1638416 | tf_op jit(solution)/shard_map/all_gather | solution.py:45
  391.4 1.8 fusion.189
  394.3 1.7 fusion.187
  396.7 1.3 copy.67
  398.0 1.3 bitcast_add_fusion.1
  399.4 1.0 copy-done.7
  400.4 1.1 bitcast_add_fusion
  401.4 45.0 %all-gather.19.cloned.1.call-done = f32[8,1,256,512]{3,2,1,0:T(8,128)} async-done(((f32[1,1,256,512]{3,2,1,0:T(8,128)}), f32[8,1,256,512]{3,2,1,0:T(8,128)}) %all-gather.19.cloned.1.call-update) | async-done | bytes 4194320 | tf_op jit(solution)/shard_map/all_gather | solution.py:59
  446.5 6.0 %fusion.125 = f32[256,512]{1,0:T(8,128)} fusion(f32[256,512]{1,0:T(8,128)} %bitcast.718, f32[1,256,1024]{1,2,0:T(8,128)} %bitcast_add_fusion, f32[1024,256]{1,0:T(8,128)S(1)} %copy-done.10, bf16[1024,800]{1,0:T(8,128)(2,1)} %all-gather.15.cloned.1.call-done, f32[8,1,256,512]{3,2,1,0:T(8,128)} %all-gather.19.cloned.1.call-done, ...), kind=kOutput, calls=%fused_computation.131 | convolution fusion | flops 341573632 | bytes 11548684 | tf_op jit(solution)/shard_map/nyf,nfe->nye/dot_general | solution.py:252
  452.5 3.4 reverse.21
  456.0 45.7 %all-gather.17.cloned.1.call-done = f32[8,1,256,512]{3,2,1,0:T(8,128)} async-done(((f32[1,1,256,512]{3,2,1,0:T(8,128)}), f32[8,1,256,512]{3,2,1,0:T(8,128)}) %all-gather.17.cloned.1.call-update) | async-done | bytes 4194320 | tf_op jit(solution)/shard_map/all_gather | solution.py:59
  501.6 4.8 multiply_reduce_fusion.1
  506.5 7.9 %convolution_convert_fusion = bf16[256,4096]{1,0:T(8,128)(2,1)} fusion(bf16[4096,2048]{1,0:T(8,128)(2,1)} %bitcast.17, bf16[256,4128]{1,0:T(8,128)(2,1)} %all-gather.13.cloned.1.call-done, f32[256,512]{1,0:T(8,128)S(1)} %get-tuple-element.277, f32[512]{0:T(512)S(1)} %convert_element_type.118, f32[256]{0:T(256)S(1)} %add_rsqrt_fusion), kind=kOutput, calls=%fused_computation.91 | convolution fusion | flops 2149842944 | bytes 13110272 | tf_op jit(solution)/shard_map/dot_general | solution.py:82
  514.4 4.4 all-to-all-start.1
  518.8 26.2 %all-to-all-done.1 = bf16[4,64,4096]{2,1,0:T(8,128)(2,1)S(1)} async-done(((bf16[4,64,4096]{2,1,0:T(8,128)(2,1)}), bf16[4,64,4096]{2,1,0:T(8,128)(2,1)S(1)}, u32[]{:S(2)}, u32[]{:S(2)}) %all-to-all-start.1) | async-done | bytes 2097184 | tf_op jit(solution)/shard_map/all_to_all | solution.py:77
  545.5 1.1 fusion.179
  (167 shorter events, 11.3 us)
Async XLA Ops:
  6.5 1.0 copy-start
  6.5 179.7 %copy-start.4 = (bf16[1,64,4096]{2,1,0:T(8,128)(2,1)S(1)}, bf16[1,64,4096]{2,1,0:T(8,128)(2,1)}, u32[]{:S(2)}) copy-start(bf16[1,64,4096]{2,1,0:T(8,128)(2,1)} %param.22) | copy-start | bytes 1572868
  6.5 129.3 %copy-start.24 = (bf16[4096]{0:T(1024)(128)(2,1)S(1)}, bf16[4096]{0:T(1024)(128)(2,1)}, u32[]{:S(2)}) copy-start(bf16[4096]{0:T(1024)(128)(2,1)} %param.29) | copy-start | bytes 24580
  6.5 180.7 %copy-start.12 = (bf16[4096,32]{0,1:T(8,128)(2,1)S(1)}, bf16[4096,32]{0,1:T(8,128)(2,1)}, u32[]{:S(2)}) copy-start(bf16[4096,32]{0,1:T(8,128)(2,1)} %param.35) | copy-start | bytes 786436
  6.5 80.9 %all-reduce.7.cloned.1.call-start = ((), (), s32[]{:S(2)}) async-start(), calls=%async_computation.8 | async-start | bytes 163840 | tf_op jit(solution)/shard_map/psum | solution.py:19
  8.3 4.3 copy-start.19
  9.5 3.1 copy-start.20
  10.3 2.3 copy-start.21
  11.5 1.2 copy-start.22
  12.6 0.6 copy-start.18
  13.2 122.5 %all-reduce.11.cloned.1.call-start = ((), (), s32[]{:S(2)}) async-start(), calls=%async_computation.10 | async-start | bytes 163840 | tf_op jit(solution)/shard_map/psum | solution.py:19
  87.5 98.0 %all-reduce.9.cloned.1.call-start = ((), (), s32[]{:S(2)}) async-start(), calls=%async_computation.9 | async-start | bytes 163840 | tf_op jit(solution)/shard_map/psum | solution.py:19
  135.8 87.5 %all-gather.13.cloned.1.call-start = ((), (), s32[]{:S(2)}) async-start(), calls=%async_computation.2 | async-start | bytes 2703360 | tf_op jit(solution)/shard_map/all_gather | solution.py:45
  135.8 55.5 %copy-start.16 = (f32[4096]{0:T(1024)}, f32[4096]{0:T(1024)S(1)}, u32[]{:S(2)}) copy-start(f32[4096]{0:T(1024)S(1)} %convert_element_type.101) | copy-start | bytes 49156
  191.4 2.9 copy-start.5
  194.3 1.6 copy-start.6
  203.3 9.9 %copy-start.26 = (f32[2,256]{1,0:T(2,128)S(1)}, f32[2,256]{1,0:T(2,128)}, u32[]{:S(2)}) copy-start(f32[2,256]{1,0:T(2,128)} %param.37) | copy-start | bytes 6148
  203.3 20.0 %copy-start.31 = (bf16[2,16,256]{2,1,0:T(8,128)(2,1)S(1)}, bf16[2,16,256]{2,1,0:T(8,128)(2,1)}, u32[]{:S(2)}) copy-start(bf16[2,16,256]{2,1,0:T(8,128)(2,1)} %param.36) | copy-start | bytes 49156
  203.3 23.4 %all-to-all-start = ((bf16[2,2048,2048]{2,1,0:T(8,128)(2,1)}), bf16[2,2048,2048]{2,1,0:T(8,128)(2,1)}, u32[]{:S(2)}, u32[]{:S(2)}) async-start(bf16[2,2048,2048]{2,1,0:T(8,128)(2,1)} %pad_maximum_fusion), calls=%async_computation | async-start | bytes 33554432 | tf_op jit(solution)/shard_map/all_to_all | solution.py:28
  213.2 63.3 %all-gather.23.cloned.1.call-start = ((), (), s32[]{:S(2)}) async-start(), calls=%async_computation.7 | async-start | bytes 2621440 | tf_op jit(solution)/shard_map/all_gather | solution.py:59
  213.9 9.4 %copy-start.29 = (f32[1,256]{1,0:T(1,128)}, f32[1,256]{1,0:T(1,128)S(1)}, u32[]{:S(2)}) copy-start(f32[1,256]{1,0:T(1,128)S(1)} %get-tuple-element.271) | copy-start | bytes 3076
  237.1 0.7 copy-start.14
  242.3 0.8 copy-start.2
  243.2 68.4 %all-gather.21.cloned.1.call-start = ((), (), s32[]{:S(2)}) async-start(), calls=%async_computation.6 | async-start | bytes 2621440 | tf_op jit(solution)/shard_map/all_gather | solution.py:59
  246.6 0.8 copy-start.3
  246.6 6.4 %copy-start.11 = (f32[2,1,128,512]{3,2,1,0:T(8,128)}, f32[2,1,128,512]{3,2,1,0:T(8,128)S(1)}, u32[]{:S(2)}) copy-start(f32[2,1,128,512]{3,2,1,0:T(8,128)S(1)} %get-tuple-element.91) | copy-start | bytes 1572868
  247.4 5.6 %copy-start.13 = (bf16[1,32,4096]{2,1,0:T(8,128)(2,1)S(1)}, bf16[1,32,4096]{2,1,0:T(8,128)(2,1)}, u32[]{:S(2)}) copy-start(bf16[1,32,4096]{2,1,0:T(8,128)(2,1)} %param.25) | copy-start | bytes 786436
  247.4 5.6 %copy-start.17 = (f32[4096]{0:T(1024)S(1)}, f32[4096]{0:T(1024)}, u32[]{:S(2)}) copy-start(f32[4096]{0:T(1024)} %copy-done.16) | copy-start | bytes 49156
  247.4 5.6 %copy-start.34 = (f32[4096]{0:T(1024)S(1)}, f32[4096]{0:T(1024)}, u32[]{:S(2)}) copy-start(f32[4096]{0:T(1024)} %get-tuple-element.224) | copy-start | bytes 49156
  247.5 143.9 %all-gather.15.cloned.1.call-start = ((), (), s32[]{:S(2)}) async-start(), calls=%async_computation.3 | async-start | bytes 1892352 | tf_op jit(solution)/shard_map/all_gather | solution.py:45
  256.8 189.7 %all-gather.19.cloned.1.call-start = ((), (), s32[]{:S(2)}) async-start(), calls=%async_computation.5 | async-start | bytes 4718592 | tf_op jit(solution)/shard_map/all_gather | solution.py:59
  279.0 35.1 %copy-start.27 = (bf16[512]{0:T(512)(128)(2,1)S(1)}, bf16[512]{0:T(512)(128)(2,1)}, u32[]{:S(2)}) copy-start(bf16[512]{0:T(512)(128)(2,1)} %param.38) | copy-start | bytes 3076
  279.0 222.6 %all-gather.17.cloned.1.call-start = ((), (), s32[]{:S(2)}) async-start(), calls=%async_computation.4 | async-start | bytes 4718592 | tf_op jit(solution)/shard_map/all_gather | solution.py:59
  314.1 77.3 %copy-start.30 = (f32[1,256]{1,0:T(1,128)S(1)}, f32[1,256]{1,0:T(1,128)}, u32[]{:S(2)}) copy-start(f32[1,256]{1,0:T(1,128)} %copy-done.29) | copy-start | bytes 3076
  314.1 77.3 %copy-start.32 = (bf16[2,16,256]{2,1,0:T(8,128)(2,1)S(1)}, bf16[2,16,256]{2,1,0:T(8,128)(2,1)}, u32[]{:S(2)}) copy-start(bf16[2,16,256]{2,1,0:T(8,128)(2,1)} %param.36) | copy-start | bytes 49156
  393.2 2.8 copy-start.9
  393.2 1.0 copy-start.28
  393.2 1.0 copy-start.33
  399.3 1.0 copy-start.7
  400.3 46.1 %copy-start.10 = (f32[1024,256]{1,0:T(8,128)S(1)}, f32[1024,256]{1,0:T(8,128)}, u32[]{:S(2)}) copy-start(f32[1024,256]{1,0:T(8,128)} %copy-done.9) | copy-start | bytes 3145732
  446.5 55.2 %copy-start.8 = (f32[1,256,1024]{1,2,0:T(8,128)S(1)}, f32[1,256,1024]{1,2,0:T(8,128)}, u32[]{:S(2)}) copy-start(f32[1,256,1024]{1,2,0:T(8,128)} %copy-done.7) | copy-start | bytes 3145732
  446.5 55.2 %copy-start.15 = (f32[256,256]{1,0:T(8,128)S(1)}, f32[256,256]{1,0:T(8,128)}, u32[]{:S(2)}) copy-start(f32[256,256]{1,0:T(8,128)} %copy-done.14) | copy-start | bytes 786436
  514.4 4.4 copy-start.25
  514.4 30.6 %all-to-all-start.1 = ((bf16[4,64,4096]{2,1,0:T(8,128)(2,1)}), bf16[4,64,4096]{2,1,0:T(8,128)(2,1)S(1)}, u32[]{:S(2)}, u32[]{:S(2)}) async-start(bf16[4,64,4096]{2,1,0:T(8,128)(2,1)} %bitcast.714), calls=%async_computation.1 | async-start | bytes 4194304 | tf_op jit(solution)/shard_map/all_to_all | solution.py:77
  518.8 26.7 %copy-start.23 = (f32[4096]{0:T(1024)S(1)}, f32[4096]{0:T(1024)}, u32[]{:S(2)}) copy-start(f32[4096]{0:T(1024)} %get-tuple-element.226) | copy-start | bytes 49156
  545.0 1.6 copy-start.1
Sparse Core Ops, SparseCore 0:
  13.4 74.0 all-reduce.6
  90.1 45.5 all-reduce.10
  138.4 47.0 all-reduce.8
  188.6 34.5 all-gather.12
  243.3 33.1 all-gather.22
  278.1 33.3 all-gather.20
  314.1 77.2 all-gather.14
  393.2 53.2 all-gather.18
  448.3 53.3 all-gather.16
